TPU v7x, 512 devices: a whole 4x4x16 slice. The times are simulated.
512 devices in a mesh: sp: 16 (over z), dp: 32 (over y, x, core).
Axes of the slice: x: 4, y: 4, z: 16, core: 2. Of those that a mesh axis runs over, the one named last changes fastest.
Arguments:
- stream_x: bfloat16 [32, 2048, 2048], P('dp', 'sp'), may hold values from -6 to 6
- stream_b: bfloat16 [32, 2048, 1024], P('dp', 'sp'), may hold values from -6 to 6
- stream_c: bfloat16 [32, 2048, 1024], P('dp', 'sp'), may hold values from -6 to 6
- gate_z: bfloat16 [32, 2048, 2048], P('dp', 'sp'), may hold values from -6 to 6
- step_raw: bfloat16 [32, 2048, 32], P('dp', 'sp'), may hold values from -4 to 3
- conv_x: bfloat16 [4, 2048], P(None, 'sp'), may hold values from -3 to 3
- conv_b: bfloat16 [4, 1024], replicated, may hold values from -3 to 3
- conv_c: bfloat16 [4, 1024], replicated, may hold values from -3 to 3
- decay_log: float32 [32], P('sp'), may hold values from -20 to 0
- norm_gain: float32 [2048], replicated, may hold values from 0.1 to 1.9
- w_out: bfloat16 [2048, 2048], P('dp'), may hold values from -0.125 to 0.125
Outputs:
- mixed: bfloat16 [32, 2048, 2048], P('dp', 'sp')
All inputs are finite; a program needn't handle non-finite values.
Results may differ from a plain program's by a relative error of at most 0.011.
Values may be sent and summed in bfloat16 or wider, within the bound.
A program may use at most 64 MiB of HBM per device.

v0:
```python
import functools
import math

import jax
import jax.numpy as jnp
from jax import lax
from jax.experimental import pallas as pl
from jax.experimental.pallas import tpu as pltpu
from jax.sharding import PartitionSpec as P

HEAD_DIM = 64
STATE = 128
NORM_EPS = 1.0
HALO = 16
LANES = 128
HOP = 2
RELAYS = (8, 11, 14, 18)
READY = 20
F32 = jnp.float32
BF16 = jnp.bfloat16


def dot(a, b, precision=None):
    return jnp.dot(a, b, preferred_element_type=F32, precision=precision)


def silu(v):
    return v / (1.0 + jnp.exp(-v))


def kernel(
    sp,
    dp,
    x_hbm,
    b_hbm,
    c_hbm,
    z_hbm,
    raw_ref,
    cx_hbm,
    cb_hbm,
    cc_hbm,
    dl_ref,
    gain_hbm,
    w_hbm,
    out_ref,
    cx_ref,
    cb_ref,
    cc_ref,
    gain_ref,
    x_v,
    b_v,
    c_v,
    z_v,
    halo_x,
    halo_b,
    halo_c,
    par,
    taps,
    wide_raw,
    ext,
    zs,
    scores,
    b_ts,
    xlow,
    inner,
    ecum,
    elast,
    wts,
    lasts,
    total,
    cact,
    local,
    a_in,
    a_out,
    b_in,
    b_out,
    normed,
    w_all,
    acc,
    in_sem,
    par_send,
    par_recv,
    last_send,
    last_recv,
    halo_send,
    halo_recv,
    a_send,
    a_recv,
    b_send,
    b_recv,
    own_sem,
    one_send,
    one_recv,
    two_send,
    two_recv,
    relay_send,
    relay_recv,
):
    tokens, inner_width = x_v.shape
    groups = b_v.shape[1] // STATE
    group_width = inner_width // groups
    pairs = group_width // LANES
    chunks = groups * pairs
    ratio = group_width // HEAD_DIM
    heads, local_heads = raw_ref.shape[1], dl_ref.shape[1]
    tap_count, tap_width = cx_ref.shape
    rows = w_hbm.shape[0]
    half_rows = rows // 2
    side = math.isqrt(dp // 2)
    cut = max(2, (3 * sp) // 8)
    middle = cut + (sp - cut + 1) // 2
    reach = max(cut, sp - cut) - 1

    pos = lax.axis_index("sp")
    me = lax.axis_index("dp")
    core = me % 2
    partner = me + 1 - 2 * core
    place = me // 2
    column, line = place % side, place // side
    following = (pos + 1) % sp
    preceding = (pos + sp - 1) % sp
    first = pos < cut

    def remote(src, dst, send, recv, target):
        return pltpu.make_async_remote_copy(
            src_ref=src,
            dst_ref=dst,
            send_sem=send,
            recv_sem=recv,
            device_id=target,
            device_id_type=pl.DeviceIdType.MESH,
        )

    def chip(axis, along, across):
        dx, dy = (along, across) if axis == 0 else (across, along)
        return ((line + dy + side) % side) * side + (column + dx + side) % side

    sources = (
        (cx_hbm, cx_ref),
        (b_hbm.at[0], b_v),
        (c_hbm.at[0], c_v),
        (x_hbm.at[0], x_v),
        (cb_hbm, cb_ref),
        (cc_hbm, cc_ref),
        (z_hbm.at[0], z_v),
        (gain_hbm, gain_ref),
    )
    loads = [
        pltpu.make_async_copy(src, dst, in_sem.at[i]) for i, (src, dst) in enumerate(sources)
    ]
    for load in loads:
        load.start()

    barrier = pltpu.get_barrier_semaphore()
    greeted = [{"sp": (pos + j) % sp} for j in range(1, sp)] + [{"dp": partner}]
    for axis in range(2):
        for i in range(1, side):
            greeted.append({"dp": 2 * chip(axis, i, 0) + core})
    for target in greeted:
        pl.semaphore_signal(
            barrier, inc=1, device_id=target, device_id_type=pl.DeviceIdType.MESH
        )

    def piece(axis, along, across):
        origin = 2 * chip(axis, along, across) + core
        start = pl.multiple_of(origin * rows + axis * half_rows, half_rows)
        return w_all.at[pl.ds(start, half_rows), :]

    own_rows = w_all.at[pl.ds(pl.multiple_of(me * rows, rows), rows), :]
    keep = pltpu.make_async_copy(w_hbm, own_rows, in_sem.at[len(sources)])
    keep.start()

    par[pos] = jnp.zeros(par.shape[1:], F32)
    wide_raw[...] = jnp.zeros(wide_raw.shape, F32)
    wide_raw[0:1, 0:local_heads] = dl_ref[...]
    par[pos, :, tap_width : tap_width + LANES] = pltpu.roll(
        wide_raw[0:8, :], pos * local_heads, 1
    )
    wide_raw[0:heads, :] = raw_ref[0].astype(F32)
    loads[0].wait()
    par[pos, 0:tap_count, 0:tap_width] = cx_ref[...].astype(F32)
    for load in loads[1:]:
        load.wait()
    keep.wait()
    pl.semaphore_wait(barrier, len(greeted))

    shares = [
        remote(
            par.at[pos],
            par.at[pos],
            par_send.at[j - 1],
            par_recv.at[j - 1],
            {"sp": (pos + j) % sp},
        )
        for j in range(1, sp)
    ]
    for copy in shares:
        copy.start()

    halos = [
        remote(
            src.at[pl.ds(tokens - HALO, HALO), :],
            dst,
            halo_send.at[i],
            halo_recv.at[i],
            {"sp": following},
        )
        for i, (src, dst) in enumerate(((x_v, halo_x), (b_v, halo_b), (c_v, halo_c)))
    ]

    @pl.when(pos < sp - 1)
    def _():
        for copy in halos:
            copy.start()

    def stage_one(axis, i):
        return remote(
            piece(axis, 0, 0),
            piece(axis, 0, 0),
            one_send.at[axis, i],
            one_recv.at[axis, i],
            {"dp": 2 * chip(axis, i, 0) + core},
        )

    def stage_two(axis, k, i):
        return remote(
            piece(axis, -k, 0),
            piece(axis, -k, 0),
            two_send.at[axis, k, i],
            two_recv.at[axis, k, i],
            {"dp": 2 * chip(axis, 0, i) + core},
        )

    def relay(axis, k, i):
        return remote(
            piece(axis, -k, -i),
            piece(axis, -k, -i),
            relay_send.at[axis, k, i],
            relay_recv.at[axis, k, i],
            {"dp": partner},
        )

    steps = sorted(range(1, side), key=lambda i: min(i, side - i))
    for i in steps:
        for axis in range(2):
            stage_one(axis, i).start()
    for i in steps:
        for axis in range(2):
            stage_two(axis, 0, i).start()
    own = remote(own_rows, own_rows, own_sem.at[0], own_sem.at[1], {"dp": partner})
    own.start()

    def spread_lines():
        for k in steps:
            for axis in range(2):
                stage_one(axis, k).wait_recv()
                for i in steps:
                    stage_two(axis, k, i).start()

    def pass_rows(step):
        if step == 0:
            for k in steps:
                for axis in range(2):
                    relay(axis, k, 0).start()
            which = 0
        else:
            which = steps[step - 1]
        for i in steps:
            for axis in range(2):
                stage_two(axis, which, i).wait_recv()
                relay(axis, which, i).start()

    raw = jnp.transpose(wide_raw[...])
    dt = jnp.maximum(raw, 0.0) + jnp.log(1.0 + jnp.exp(-jnp.abs(raw)))
    down = lax.broadcasted_iota(jnp.int32, (tokens, tokens), 0)
    across_tokens = lax.broadcasted_iota(jnp.int32, (tokens, tokens), 1)
    causal = down >= across_tokens
    left_half = lax.broadcasted_iota(jnp.int32, (tokens, LANES), 1) < HEAD_DIM
    left_row = left_half[0:1, :]
    for g in range(groups):
        taps[g, 0:tap_count, group_width : group_width + STATE] = cb_ref[
            :, g * STATE : (g + 1) * STATE
        ].astype(F32)
        taps[g, 0:tap_count, group_width + STATE : group_width + 2 * STATE] = cc_ref[
            :, g * STATE : (g + 1) * STATE
        ].astype(F32)
        zs[g] = silu(z_v[:, g * group_width : (g + 1) * group_width].astype(F32))

    @pl.when(pos == 0)
    def _():
        ext[:, 0:8, :] = jnp.zeros((groups, 8, ext.shape[2]), F32)

    @pl.when((pos == 0) | (pos == cut))
    def _():
        a_in[...] = jnp.zeros(a_in.shape, BF16)

    @pl.when(pos > 0)
    def _():
        for copy in halos:
            copy.wait_recv()
        for g in range(groups):
            wide = slice(g * group_width, (g + 1) * group_width)
            thin = slice(g * STATE, (g + 1) * STATE)
            ext[g, 0:8, 0:group_width] = halo_x[:, wide].astype(F32)[HALO - 8 :]
            ext[g, 0:8, group_width : group_width + STATE] = halo_b[:, thin].astype(F32)[
                HALO - 8 :
            ]
            ext[g, 0:8, group_width + STATE :] = halo_c[:, thin].astype(F32)[HALO - 8 :]

    def conv(g, source, at):
        columns = slice(at, at + LANES)
        ext[g, 8 : 8 + tokens, columns] = source.astype(F32)
        summed = taps[g, 0:1, columns] * ext[g, 9 - tap_count : 9 - tap_count + tokens, columns]
        for k in range(1, tap_count):
            start = 9 - tap_count + k
            summed = summed + taps[g, k : k + 1, columns] * ext[g, start : start + tokens, columns]
        return silu(summed).astype(BF16)

    for g in range(groups):
        thin = slice(g * STATE, (g + 1) * STATE)
        b_act = conv(g, b_v[:, thin], group_width)
        c_act = conv(g, c_v[:, thin], group_width + STATE)
        cact[g] = c_act
        b_t = jnp.transpose(b_act)
        b_ts[g] = b_t
        scores[g] = dot(c_act, b_t)

    for copy in shares:
        copy.wait_recv()
    rates = par[0, 0:1, tap_width : tap_width + LANES]
    for s in range(1, sp):
        rates = rates + par[s, 0:1, tap_width : tap_width + LANES]
    log_decay = dt * (-jnp.exp(rates))
    cum = dot(jnp.where(causal, 1.0, 0.0).astype(F32), log_decay, lax.Precision.HIGHEST)
    cum_t = jnp.transpose(cum)
    lasts[0] = jnp.broadcast_to(cum[tokens - 1 : tokens, :], lasts.shape[1:])

    def tell(d):
        target = jnp.where(first, pos + sp - d, pos + d) % sp
        return remote(
            lasts.at[0], lasts.at[d], last_send.at[d], last_recv.at[d], {"sp": target}
        )

    def tells(d):
        return (first & (pos >= d)) | (jnp.logical_not(first) & (pos + d < sp))

    def hears(d):
        return (first & (pos + d < cut)) | (jnp.logical_not(first) & (pos - d >= cut))

    for d in range(1, reach + 1):

        @pl.when(tells(d))
        def _():
            tell(d).start()

    for chunk in range(chunks):
        begin = chunk * LANES
        g, at = begin // group_width, begin % group_width
        s, off = begin // tap_width, begin % tap_width
        taps[g, 0:tap_count, at : at + LANES] = par[s, 0:tap_count, off : off + LANES]

    def chain(j):
        return remote(a_out.at[j], a_in.at[j], a_send.at[j], a_recv.at[j], {"sp": following})

    def cross(j):
        return remote(a_out.at[j], b_in.at[j], a_send.at[j], b_recv.at[j], {"sp": following})

    def back(j):
        return remote(b_out.at[j], b_in.at[j], b_send.at[j], b_recv.at[j], {"sp": preceding})

    def carry_up(j):
        return remote(b_in.at[j], b_in.at[j], b_send.at[j], b_recv.at[j], {"sp": following})

    def carry_down(j):
        return remote(b_in.at[j], b_in.at[j], b_send.at[j], b_recv.at[j], {"sp": preceding})

    carries_up = (pos >= cut) & (pos < middle - 1)
    carries_down = pos > middle

    for g in range(groups):
        b_t = b_ts[g]
        for p in range(pairs):
            j = g * pairs + p
            columns = slice(j * LANES, (j + 1) * LANES)
            local_columns = slice(p * LANES, (p + 1) * LANES)
            x_act = conv(g, x_v[:, columns], p * LANES).astype(F32)
            h = g * ratio + 2 * p
            step = jnp.where(left_half, dt[:, h : h + 1], dt[:, h + 1 : h + 2])
            both = jnp.where(left_half, cum[:, h : h + 1], cum[:, h + 1 : h + 2])
            x_dt = x_act * step
            xlow[g, :, local_columns] = x_dt.astype(BF16)
            ecum[g, :, local_columns] = jnp.exp(both)
            last = both[tokens - 1 : tokens, :]
            elast[j, 0:1, :] = jnp.exp(last)
            x_tail = (x_dt * jnp.exp(last - both)).astype(BF16)
            mine = dot(b_t, x_tail)
            local[j] = mine

            @pl.when((pos == 0) | (pos == cut))
            def _():
                a_out[j] = local[j].astype(BF16)
                chain(j).start()

            @pl.when(pos == cut - 1)
            def _():
                b_out[j] = local[j].astype(BF16)
                back(j).start()

    def weigh():
        total[...] = jnp.zeros(total.shape, F32)
        for d in range(1, reach + 1):

            @pl.when(hears(d))
            def _():
                tell(d).wait_recv()
                total[...] += lasts[d]

        weight = jnp.exp(total[0:1, :])
        for j in range(chunks):
            wts[j, 0:1, :] = jnp.where(
                left_row, weight[:, 2 * j : 2 * j + 1], weight[:, 2 * j + 1 : 2 * j + 2]
            )

    def step_a(j):
        @pl.when((pos != 0) & (pos != cut))
        def _():
            chain(j).wait_recv()

            @pl.when(pos < sp - 1)
            def _():
                a_out[j] = (a_in[j].astype(F32) * elast[j, 0:1, :] + local[j]).astype(BF16)

            @pl.when((pos != cut - 1) & (pos < sp - 1))
            def _():
                chain(j).start()

            @pl.when(pos == cut - 1)
            def _():
                cross(j).start()

    def step_b(j):
        @pl.when(pos < cut - 1)
        def _():
            back(j).wait_recv()
            b_out[j] = (b_in[j].astype(F32) + wts[j, 0:1, :] * local[j]).astype(BF16)
            back(j).start()

        @pl.when(pos >= cut)
        def _():
            carry_up(j).wait_recv()

            @pl.when(carries_up)
            def _():
                carry_up(j).start()

            @pl.when(carries_down)
            def _():
                carry_down(j).start()

    lag_a = jnp.where(first, HOP * pos, HOP * (pos - cut))
    lag_b = jnp.where(
        first,
        HOP * (cut - 1 - pos),
        jnp.where(pos < middle, HOP * pos, HOP * (cut + sp - 1 - pos)),
    )

    def flows(s):
        @pl.when((s >= lag_a) & (s < lag_a + groups))
        def _():
            for p in range(pairs):
                step_a((s - lag_a) * pairs + p)

        @pl.when((s >= lag_b) & (s < lag_b + groups))
        def _():
            for p in range(pairs):
                step_b((s - lag_b) * pairs + p)

    def inside(g):
        for p in range(pairs):
            local_columns = slice(p * LANES, (p + 1) * LANES)
            x_low = xlow[g, :, local_columns]
            h = g * ratio + 2 * p
            parts = []
            for i in range(2):
                gap = cum[:, h + i : h + i + 1] - cum_t[h + i : h + i + 1, :]
                weight = scores[g] * jnp.exp(jnp.where(causal, gap, -jnp.inf))
                parts.append(dot(weight.astype(BF16), x_low))
            inner[g, :, local_columns] = jnp.where(left_half, parts[0], parts[1])

    spread_lines()

    @pl.when(first)
    def _():
        weigh()

    for s in range(groups):
        flows(s)
        inside(s)

    @pl.when(jnp.logical_not(first))
    def _():
        weigh()

    sum_down = lax.broadcasted_iota(jnp.int32, (group_width, group_width), 0) // HEAD_DIM
    sum_across = lax.broadcasted_iota(jnp.int32, (group_width, group_width), 1) // HEAD_DIM
    averager = jnp.where(sum_down == sum_across, 1.0 / HEAD_DIM, 0.0).astype(BF16)

    def finish(g):
        entering = []
        for p in range(pairs):
            j = g * pairs + p
            more = jnp.where(first, 0.0, wts[j, 0:1, :] * b_in[j].astype(F32))
            entering.append((a_in[j].astype(F32) + more).astype(BF16))
        carried = dot(cact[g], jnp.concatenate(entering, axis=1))
        core_out = (inner[g] + ecum[g] * carried).astype(BF16)
        value = core_out.astype(F32) * zs[g]
        square = value * value
        high = square.astype(BF16)
        low = (square - high.astype(F32)).astype(BF16)
        mean = dot(high, averager) + dot(low, averager)
        gain = gain_ref[0:1, pl.ds(pl.multiple_of(g * group_width, group_width), group_width)]
        normed[g] = (value * lax.rsqrt(mean + NORM_EPS) * gain).astype(BF16)

    def project(g):
        start = pl.multiple_of(g * group_width, group_width)
        part = dot(normed[g], w_all[pl.ds(start, group_width), :])

        @pl.when(g == 0)
        def _():
            acc[...] = part

        @pl.when(g > 0)
        def _():
            acc[...] += part

    lag_f = jnp.maximum(jnp.maximum(lag_a, lag_b), groups)
    lag_p = jnp.maximum(lag_f, READY)

    def slot(s, carry):
        flows(s)
        for step, at in enumerate(RELAYS[:side]):

            @pl.when(s == at)
            def _():
                pass_rows(step)

        @pl.when(s == READY)
        def _():
            own.wait_recv()
            for axis in range(2):
                for k in range(side):
                    for i in range(side):
                        if k or i:
                            relay(axis, k, i).wait_recv()

        @pl.when((s >= lag_f) & (s < lag_f + groups))
        def _():
            finish(s - lag_f)

        @pl.when((s >= lag_p) & (s < lag_p + groups))
        def _():
            project(s - lag_p)

        return carry

    lax.fori_loop(groups, lag_p + groups, slot, 0)
    out_ref[0] = acc[...].astype(BF16)

    own.wait_send()
    for copy in shares:
        copy.wait_send()
    for axis in range(2):
        for i in steps:
            stage_one(axis, i).wait_send()
            for k in range(side):
                stage_two(axis, k, i).wait_send()
        for k in range(side):
            for i in range(side):
                if k or i:
                    relay(axis, k, i).wait_send()
    for d in range(1, reach + 1):

        @pl.when(tells(d))
        def _():
            tell(d).wait_send()

    @pl.when(pos < sp - 1)
    def _():
        for copy in halos:
            copy.wait_send()
        for j in range(chunks):
            chain(j).wait_send()

    @pl.when(first | carries_up | carries_down)
    def _():
        for j in range(chunks):
            back(j).wait_send()


def body(
    sp,
    dp,
    stream_x,
    stream_b,
    stream_c,
    gate_z,
    step_raw,
    conv_x,
    conv_b,
    conv_c,
    decay_log,
    norm_gain,
    w_out,
):
    tokens, width = stream_x.shape[1:]
    state_width = stream_b.shape[2]
    groups = state_width // STATE
    group_width = width // groups
    chunks = width // LANES
    columns = w_out.shape[1]
    side = math.isqrt(dp // 2)
    vmem = pl.BlockSpec(memory_space=pltpu.VMEM)
    anywhere = pl.BlockSpec(memory_space=pl.ANY)
    dma = pltpu.SemaphoreType.DMA
    return pl.pallas_call(
        functools.partial(kernel, sp, dp),
        out_shape=jax.ShapeDtypeStruct((1, tokens, columns), BF16),
        in_specs=[anywhere] * 4 + [vmem] + [anywhere] * 3 + [vmem] + [anywhere] * 2,
        out_specs=vmem,
        scratch_shapes=[
            pltpu.VMEM(conv_x.shape, BF16),
            pltpu.VMEM(conv_b.shape, BF16),
            pltpu.VMEM(conv_c.shape, BF16),
            pltpu.VMEM((1, width), F32),
            pltpu.VMEM((tokens, width), BF16),
            pltpu.VMEM((tokens, state_width), BF16),
            pltpu.VMEM((tokens, state_width), BF16),
            pltpu.VMEM((tokens, width), BF16),
            pltpu.VMEM((HALO, width), BF16),
            pltpu.VMEM((HALO, state_width), BF16),
            pltpu.VMEM((HALO, state_width), BF16),
            pltpu.VMEM((sp, 8, conv_x.shape[1] + LANES), F32),
            pltpu.VMEM((groups, 8, group_width + 2 * STATE), F32),
            pltpu.VMEM((LANES, tokens), F32),
            pltpu.VMEM((groups, tokens + 8, group_width + 2 * STATE), F32),
            pltpu.VMEM((groups, tokens, group_width), F32),
            pltpu.VMEM((groups, tokens, tokens), F32),
            pltpu.VMEM((groups, STATE, tokens), BF16),
            pltpu.VMEM((groups, tokens, group_width), BF16),
            pltpu.VMEM((groups, tokens, group_width), F32),
            pltpu.VMEM((groups, tokens, group_width), F32),
            pltpu.VMEM((chunks, 8, LANES), F32),
            pltpu.VMEM((chunks, 8, LANES), F32),
            pltpu.VMEM((sp, 8, LANES), F32),
            pltpu.VMEM((8, LANES), F32),
            pltpu.VMEM((groups, tokens, STATE), BF16),
            pltpu.VMEM((chunks, STATE, LANES), F32),
            pltpu.VMEM((chunks, STATE, LANES), BF16),
            pltpu.VMEM((chunks, STATE, LANES), BF16),
            pltpu.VMEM((chunks, STATE, LANES), BF16),
            pltpu.VMEM((chunks, STATE, LANES), BF16),
            pltpu.VMEM((groups, tokens, group_width), BF16),
            pltpu.VMEM((width, columns), BF16),
            pltpu.VMEM((tokens, columns), F32),
            dma((9,)),
            dma((sp,)),
            dma((sp,)),
            dma((sp,)),
            dma((sp,)),
            dma((3,)),
            dma((3,)),
            dma((chunks,)),
            dma((chunks,)),
            dma((chunks,)),
            dma((chunks,)),
            dma((2,)),
            dma((2, side)),
            dma((2, side)),
            dma((2, side, side)),
            dma((2, side, side)),
            dma((2, side, side)),
            dma((2, side, side)),
        ],
        compiler_params=pltpu.CompilerParams(
            collective_id=0, has_side_effects=True, vmem_limit_bytes=60 * 1024 * 1024
        ),
    )(
        stream_x,
        stream_b,
        stream_c,
        gate_z,
        jnp.swapaxes(step_raw, 1, 2),
        conv_x,
        conv_b,
        conv_c,
        decay_log.reshape(1, -1),
        norm_gain.reshape(1, -1),
        w_out,
    )


def solution(mesh):
    placed = (
        P("dp", "sp", None),
        P("dp", "sp", None),
        P("dp", "sp", None),
        P("dp", "sp", None),
        P("dp", "sp", None),
        P(None, "sp"),
        P(),
        P(),
        P("sp"),
        P(),
        P("dp", None),
    )
    return jax.shard_map(
        functools.partial(body, mesh.shape["sp"], mesh.shape["dp"]),
        mesh=mesh,
        in_specs=placed,
        out_specs=P("dp", "sp", None),
        check_vma=False,
    )
```

profile of v0, /device:TPU:1, one launch (start us, length us, event | category | flops | bytes accessed | tf_op | source)
XLA Modules:
  0.0 71.7 jit_solution(4123946512342167123)
XLA Ops:
  0.0 69.8 %shard_map.109 = bf16[1,128,2048]{2,1,0:T(8,128)(2,1)} custom-call(bf16[1,128,2048]{2,1,0:T(8,128)(2,1)} %x_hbm.1, bf16[1,128,1024]{2,1,0:T(8,128)(2,1)} %b_hbm.1, bf16[1,128,1024]{2,1,0:T(8,128)(2,1)} %c_hbm.1, bf16[1,128,2048]{2,1,0:T(8,128)(2,1)} %z_hbm.1, bf16[1,32,128]{2,1,0:T(8,128)(2,1)} %bitcast.3, bf16[4,128]{1,0:T(4,128)(2,1)} %cx_hbm.1, ...), custom_call_target="tpu_custom_call" | custom-call | tf_op jit(solution)/shard_map/pallas_call | solution.py:625
  69.8 1.9 %copy.13 = bf16[1,128,2048]{2,1,0:T(8,128)(2,1)} copy(bf16[1,128,2048]{2,1,0:T(8,128)(2,1)} %shard_map.109) | data formatting | bytes 1048576
where the time goes:
time: 71.9 us; the launch traced here: 71.7 us
  Pallas kernels  69.8 us (97%)
  local copies, waits for them, and re-layouts  1.88 us (3%)
    pallas_call x1, Pallas kernels, body(): pl.pallas_call(functools.partial(kernel, sp, dp), out_shape=jax.ShapeDtyp...  69.8 us
    unnamed x1, local copies, waits for them, and re-layouts  1.88 us

commit v1 on v0

--- a/solution.py
+++ b/solution.py
@@ -11,11 +11,10 @@
 HEAD_DIM = 64
 STATE = 128
 NORM_EPS = 1.0
-HALO = 16
+HALO = 8
 LANES = 128
 HOP = 2
 RELAYS = (8, 11, 14, 18)
-READY = 20
 F32 = jnp.float32
 BF16 = jnp.bfloat16
 
@@ -35,14 +34,16 @@
     b_hbm,
     c_hbm,
     z_hbm,
-    raw_ref,
+    raw_hbm,
     cx_hbm,
     cb_hbm,
     cc_hbm,
-    dl_ref,
+    dl_hbm,
     gain_hbm,
     w_hbm,
     out_ref,
+    raw_ref,
+    dl_ref,
     cx_ref,
     cb_ref,
     cc_ref,
@@ -55,13 +56,14 @@
     halo_b,
     halo_c,
     par,
+    tile,
     taps,
     wide_raw,
     ext,
     zs,
     scores,
     b_ts,
-    xlow,
+    xact,
     inner,
     ecum,
     elast,
@@ -76,7 +78,6 @@
     b_out,
     normed,
     w_all,
-    acc,
     in_sem,
     par_send,
     par_recv,
@@ -102,7 +103,7 @@
     pairs = group_width // LANES
     chunks = groups * pairs
     ratio = group_width // HEAD_DIM
-    heads, local_heads = raw_ref.shape[1], dl_ref.shape[1]
+    heads, local_heads = raw_ref.shape[0], dl_ref.shape[1]
     tap_count, tap_width = cx_ref.shape
     rows = w_hbm.shape[0]
     half_rows = rows // 2
@@ -135,8 +136,20 @@
         dx, dy = (along, across) if axis == 0 else (across, along)
         return ((line + dy + side) % side) * side + (column + dx + side) % side
 
+    barrier = pltpu.get_barrier_semaphore()
+    greeted = [{"sp": (pos + j) % sp} for j in range(1, sp)] + [{"dp": partner}]
+    for axis in range(2):
+        for i in range(1, side):
+            greeted.append({"dp": 2 * chip(axis, i, 0) + core})
+    for target in greeted:
+        pl.semaphore_signal(
+            barrier, inc=1, device_id=target, device_id_type=pl.DeviceIdType.MESH
+        )
+
     sources = (
         (cx_hbm, cx_ref),
+        (dl_hbm, dl_ref),
+        (raw_hbm.at[0], raw_ref),
         (b_hbm.at[0], b_v),
         (c_hbm.at[0], c_v),
         (x_hbm.at[0], x_v),
@@ -151,16 +164,6 @@
     for load in loads:
         load.start()
 
-    barrier = pltpu.get_barrier_semaphore()
-    greeted = [{"sp": (pos + j) % sp} for j in range(1, sp)] + [{"dp": partner}]
-    for axis in range(2):
-        for i in range(1, side):
-            greeted.append({"dp": 2 * chip(axis, i, 0) + core})
-    for target in greeted:
-        pl.semaphore_signal(
-            barrier, inc=1, device_id=target, device_id_type=pl.DeviceIdType.MESH
-        )
-
     def piece(axis, along, across):
         origin = 2 * chip(axis, along, across) + core
         start = pl.multiple_of(origin * rows + axis * half_rows, half_rows)
@@ -170,19 +173,39 @@
     keep = pltpu.make_async_copy(w_hbm, own_rows, in_sem.at[len(sources)])
     keep.start()
 
-    par[pos] = jnp.zeros(par.shape[1:], F32)
     wide_raw[...] = jnp.zeros(wide_raw.shape, F32)
+    for load in loads[0:3]:
+        load.wait()
     wide_raw[0:1, 0:local_heads] = dl_ref[...]
-    par[pos, :, tap_width : tap_width + LANES] = pltpu.roll(
-        wide_raw[0:8, :], pos * local_heads, 1
-    )
-    wide_raw[0:heads, :] = raw_ref[0].astype(F32)
-    loads[0].wait()
-    par[pos, 0:tap_count, 0:tap_width] = cx_ref[...].astype(F32)
-    for load in loads[1:]:
+    decays = pltpu.roll(wide_raw[0:8, :], pos * local_heads, 1)[0:1, :]
+    tile[...] = jnp.zeros(tile.shape, F32)
+    tile[0:tap_count, :] = cx_ref[...].astype(F32)
+    for i in range(3):
+        part = decays.astype(BF16).astype(F32)
+        tile[tap_count + i : tap_count + i + 1, :] = part
+        decays = decays - part
+    par[pos] = tile[...].astype(BF16)
+    wide_raw[0:heads, :] = raw_ref[...].astype(F32)
+    for load in loads[3:]:
         load.wait()
     keep.wait()
     pl.semaphore_wait(barrier, len(greeted))
+
+    halos = [
+        remote(
+            src.at[pl.ds(tokens - HALO, HALO), :],
+            dst,
+            halo_send.at[i],
+            halo_recv.at[i],
+            {"sp": following},
+        )
+        for i, (src, dst) in enumerate(((x_v, halo_x), (b_v, halo_b), (c_v, halo_c)))
+    ]
+
+    @pl.when(pos < sp - 1)
+    def _():
+        for copy in halos:
+            copy.start()
 
     shares = [
         remote(
@@ -196,22 +219,6 @@
     ]
     for copy in shares:
         copy.start()
-
-    halos = [
-        remote(
-            src.at[pl.ds(tokens - HALO, HALO), :],
-            dst,
-            halo_send.at[i],
-            halo_recv.at[i],
-            {"sp": following},
-        )
-        for i, (src, dst) in enumerate(((x_v, halo_x), (b_v, halo_b), (c_v, halo_c)))
-    ]
-
-    @pl.when(pos < sp - 1)
-    def _():
-        for copy in halos:
-            copy.start()
 
     def stage_one(axis, i):
         return remote(
@@ -301,11 +308,9 @@
         for g in range(groups):
             wide = slice(g * group_width, (g + 1) * group_width)
             thin = slice(g * STATE, (g + 1) * STATE)
-            ext[g, 0:8, 0:group_width] = halo_x[:, wide].astype(F32)[HALO - 8 :]
-            ext[g, 0:8, group_width : group_width + STATE] = halo_b[:, thin].astype(F32)[
-                HALO - 8 :
-            ]
-            ext[g, 0:8, group_width + STATE :] = halo_c[:, thin].astype(F32)[HALO - 8 :]
+            ext[g, 0:8, 0:group_width] = halo_x[:, wide].astype(F32)
+            ext[g, 0:8, group_width : group_width + STATE] = halo_b[:, thin].astype(F32)
+            ext[g, 0:8, group_width + STATE :] = halo_c[:, thin].astype(F32)
 
     def conv(g, source, at):
         columns = slice(at, at + LANES)
@@ -327,13 +332,18 @@
 
     for copy in shares:
         copy.wait_recv()
-    rates = par[0, 0:1, tap_width : tap_width + LANES]
+    gathered = par[0].astype(F32)
     for s in range(1, sp):
-        rates = rates + par[s, 0:1, tap_width : tap_width + LANES]
+        gathered = gathered + par[s].astype(F32)
+    rates = gathered[tap_count : tap_count + 1, :]
+    for i in range(1, 3):
+        rates = rates + gathered[tap_count + i : tap_count + i + 1, :]
     log_decay = dt * (-jnp.exp(rates))
     cum = dot(jnp.where(causal, 1.0, 0.0).astype(F32), log_decay, lax.Precision.HIGHEST)
     cum_t = jnp.transpose(cum)
-    lasts[0] = jnp.broadcast_to(cum[tokens - 1 : tokens, :], lasts.shape[1:])
+    last = cum[tokens - 1 : tokens, :]
+    lasts[0] = jnp.broadcast_to(last, lasts.shape[1:])
+    tail = dt * jnp.exp(last - cum)
 
     def tell(d):
         target = jnp.where(first, pos + sp - d, pos + d) % sp
@@ -356,8 +366,8 @@
     for chunk in range(chunks):
         begin = chunk * LANES
         g, at = begin // group_width, begin % group_width
-        s, off = begin // tap_width, begin % tap_width
-        taps[g, 0:tap_count, at : at + LANES] = par[s, 0:tap_count, off : off + LANES]
+        s = begin // tap_width
+        taps[g, 0:tap_count, at : at + LANES] = par[s].astype(F32)[0:tap_count, :]
 
     def chain(j):
         return remote(a_out.at[j], a_in.at[j], a_send.at[j], a_recv.at[j], {"sp": following})
@@ -377,34 +387,45 @@
     carries_up = (pos >= cut) & (pos < middle - 1)
     carries_down = pos > middle
 
-    for g in range(groups):
+    def spread_rows(rows_ref, values):
+        for j in range(chunks):
+            rows_ref[j, 0:1, :] = jnp.where(
+                left_row, values[:, 2 * j : 2 * j + 1], values[:, 2 * j + 1 : 2 * j + 2]
+            )
+
+    def spread_columns(values, h):
+        return jnp.where(left_half, values[:, h : h + 1], values[:, h + 1 : h + 2])
+
+    def states(g):
         b_t = b_ts[g]
         for p in range(pairs):
             j = g * pairs + p
-            columns = slice(j * LANES, (j + 1) * LANES)
-            local_columns = slice(p * LANES, (p + 1) * LANES)
-            x_act = conv(g, x_v[:, columns], p * LANES).astype(F32)
-            h = g * ratio + 2 * p
-            step = jnp.where(left_half, dt[:, h : h + 1], dt[:, h + 1 : h + 2])
-            both = jnp.where(left_half, cum[:, h : h + 1], cum[:, h + 1 : h + 2])
-            x_dt = x_act * step
-            xlow[g, :, local_columns] = x_dt.astype(BF16)
-            ecum[g, :, local_columns] = jnp.exp(both)
-            last = both[tokens - 1 : tokens, :]
-            elast[j, 0:1, :] = jnp.exp(last)
-            x_tail = (x_dt * jnp.exp(last - both)).astype(BF16)
-            mine = dot(b_t, x_tail)
-            local[j] = mine
-
-            @pl.when((pos == 0) | (pos == cut))
-            def _():
-                a_out[j] = local[j].astype(BF16)
-                chain(j).start()
-
-            @pl.when(pos == cut - 1)
-            def _():
-                b_out[j] = local[j].astype(BF16)
-                back(j).start()
+            x_act = conv(g, x_v[:, j * LANES : (j + 1) * LANES], p * LANES)
+            xact[g, :, p * LANES : (p + 1) * LANES] = x_act
+            x_tail = (x_act.astype(F32) * spread_columns(tail, 2 * j)).astype(BF16)
+            local[j] = dot(b_t, x_tail)
+
+    def begin_flows(some, which):
+        @pl.when((core == which) & ((pos == 0) | (pos == cut)))
+        def _():
+            for g in some:
+                for j in range(g * pairs, (g + 1) * pairs):
+                    a_out[j] = local[j].astype(BF16)
+                    chain(j).start()
+
+        @pl.when((core == which) & (pos == cut - 1))
+        def _():
+            for g in some:
+                for j in range(g * pairs, (g + 1) * pairs):
+                    b_out[j] = local[j].astype(BF16)
+                    back(j).start()
+
+    for number, some in enumerate(([0], range(1, groups // 2), range(groups // 2, groups))):
+        for g in some:
+            states(g)
+        if number == 0:
+            spread_rows(elast, jnp.exp(last))
+        begin_flows(some, 0)
 
     def weigh():
         total[...] = jnp.zeros(total.shape, F32)
@@ -415,11 +436,7 @@
                 tell(d).wait_recv()
                 total[...] += lasts[d]
 
-        weight = jnp.exp(total[0:1, :])
-        for j in range(chunks):
-            wts[j, 0:1, :] = jnp.where(
-                left_row, weight[:, 2 * j : 2 * j + 1], weight[:, 2 * j + 1 : 2 * j + 2]
-            )
+        spread_rows(wts, jnp.exp(total[0:1, :]))
 
     def step_a(j):
         @pl.when((pos != 0) & (pos != cut))
@@ -478,28 +495,31 @@
     def inside(g):
         for p in range(pairs):
             local_columns = slice(p * LANES, (p + 1) * LANES)
-            x_low = xlow[g, :, local_columns]
             h = g * ratio + 2 * p
+            x_dt = xact[g, :, local_columns].astype(F32) * spread_columns(dt, h)
+            x_low = x_dt.astype(BF16)
             parts = []
+            spread = []
             for i in range(2):
-                gap = cum[:, h + i : h + i + 1] - cum_t[h + i : h + i + 1, :]
+                spread.append(jnp.broadcast_to(cum[:, h + i : h + i + 1], (tokens, LANES)))
+                gap = spread[i] - cum_t[h + i : h + i + 1, :]
                 weight = scores[g] * jnp.exp(jnp.where(causal, gap, -jnp.inf))
                 parts.append(dot(weight.astype(BF16), x_low))
             inner[g, :, local_columns] = jnp.where(left_half, parts[0], parts[1])
-
-    spread_lines()
-
-    @pl.when(first)
-    def _():
-        weigh()
+            ecum[g, :, local_columns] = jnp.exp(jnp.where(left_half, spread[0], spread[1]))
 
     for s in range(groups):
+        if s == 0 or s == groups // 2:
+
+            @pl.when(first & ((pos >= cut - 2) if s == 0 else (pos < cut - 2)))
+            def _():
+                weigh()
+
         flows(s)
         inside(s)
-
-    @pl.when(jnp.logical_not(first))
-    def _():
-        weigh()
+        if s == 0:
+            spread_lines()
+    begin_flows(range(groups), 1)
 
     sum_down = lax.broadcasted_iota(jnp.int32, (group_width, group_width), 0) // HEAD_DIM
     sum_across = lax.broadcasted_iota(jnp.int32, (group_width, group_width), 1) // HEAD_DIM
@@ -521,20 +541,8 @@
         gain = gain_ref[0:1, pl.ds(pl.multiple_of(g * group_width, group_width), group_width)]
         normed[g] = (value * lax.rsqrt(mean + NORM_EPS) * gain).astype(BF16)
 
-    def project(g):
-        start = pl.multiple_of(g * group_width, group_width)
-        part = dot(normed[g], w_all[pl.ds(start, group_width), :])
-
-        @pl.when(g == 0)
-        def _():
-            acc[...] = part
-
-        @pl.when(g > 0)
-        def _():
-            acc[...] += part
-
     lag_f = jnp.maximum(jnp.maximum(lag_a, lag_b), groups)
-    lag_p = jnp.maximum(lag_f, READY)
+    slots = jnp.maximum(lag_f + groups, RELAYS[side - 1] + 1)
 
     def slot(s, carry):
         flows(s)
@@ -544,27 +552,28 @@
             def _():
                 pass_rows(step)
 
-        @pl.when(s == READY)
-        def _():
-            own.wait_recv()
-            for axis in range(2):
-                for k in range(side):
-                    for i in range(side):
-                        if k or i:
-                            relay(axis, k, i).wait_recv()
+        @pl.when(jnp.logical_not(first) & (s == lag_f))
+        def _():
+            weigh()
 
         @pl.when((s >= lag_f) & (s < lag_f + groups))
         def _():
             finish(s - lag_f)
 
-        @pl.when((s >= lag_p) & (s < lag_p + groups))
-        def _():
-            project(s - lag_p)
-
         return carry
 
-    lax.fori_loop(groups, lag_p + groups, slot, 0)
-    out_ref[0] = acc[...].astype(BF16)
+    lax.fori_loop(groups, slots, slot, 0)
+
+    own.wait_recv()
+    for axis in range(2):
+        for k in range(side):
+            for i in range(side):
+                if k or i:
+                    relay(axis, k, i).wait_recv()
+    result = dot(normed[0], w_all[0:group_width, :])
+    for g in range(1, groups):
+        result += dot(normed[g], w_all[g * group_width : (g + 1) * group_width, :])
+    out_ref[0] = result.astype(BF16)
 
     own.wait_send()
     for copy in shares:
@@ -625,9 +634,11 @@
     return pl.pallas_call(
         functools.partial(kernel, sp, dp),
         out_shape=jax.ShapeDtypeStruct((1, tokens, columns), BF16),
-        in_specs=[anywhere] * 4 + [vmem] + [anywhere] * 3 + [vmem] + [anywhere] * 2,
+        in_specs=[anywhere] * 11,
         out_specs=vmem,
         scratch_shapes=[
+            pltpu.VMEM((step_raw.shape[2], tokens), BF16),
+            pltpu.VMEM((1, decay_log.shape[0]), F32),
             pltpu.VMEM(conv_x.shape, BF16),
             pltpu.VMEM(conv_b.shape, BF16),
             pltpu.VMEM(conv_c.shape, BF16),
@@ -639,7 +650,8 @@
             pltpu.VMEM((HALO, width), BF16),
             pltpu.VMEM((HALO, state_width), BF16),
             pltpu.VMEM((HALO, state_width), BF16),
-            pltpu.VMEM((sp, 8, conv_x.shape[1] + LANES), F32),
+            pltpu.VMEM((sp, 8, LANES), BF16),
+            pltpu.VMEM((8, LANES), F32),
             pltpu.VMEM((groups, 8, group_width + 2 * STATE), F32),
             pltpu.VMEM((LANES, tokens), F32),
             pltpu.VMEM((groups, tokens + 8, group_width + 2 * STATE), F32),
@@ -661,8 +673,7 @@
             pltpu.VMEM((chunks, STATE, LANES), BF16),
             pltpu.VMEM((groups, tokens, group_width), BF16),
             pltpu.VMEM((width, columns), BF16),
-            pltpu.VMEM((tokens, columns), F32),
-            dma((9,)),
+            dma((11,)),
             dma((sp,)),
             dma((sp,)),
             dma((sp,)),

time: 71.9 us -> 65 us (0.904)
  the two profiles are of different devices: /device:TPU:1 before, /device:TPU:356 now
where the time goes in v1:
time: 65 us; the launch traced here: 64.8 us
  Pallas kernels  62.9 us (97%)
  local copies, waits for them, and re-layouts  1.88 us (3%)
    pallas_call x1, Pallas kernels, body(): pl.pallas_call(functools.partial(kernel, sp, dp), out_shape=jax.ShapeDtyp...  62.9 us
    unnamed x1, local copies, waits for them, and re-layouts  1.88 us

profile of v1, /device:TPU:356, one launch (start us, length us, event | category | flops | bytes accessed | tf_op | source)
XLA Modules:
  0.0 64.8 jit_solution(6797783660895706497)
XLA Ops:
  0.0 62.9 %shard_map.109 = bf16[1,128,2048]{2,1,0:T(8,128)(2,1)} custom-call(bf16[1,128,2048]{2,1,0:T(8,128)(2,1)} %x_hbm.1, bf16[1,128,1024]{2,1,0:T(8,128)(2,1)} %b_hbm.1, bf16[1,128,1024]{2,1,0:T(8,128)(2,1)} %c_hbm.1, bf16[1,128,2048]{2,1,0:T(8,128)(2,1)} %z_hbm.1, bf16[1,32,128]{2,1,0:T(8,128)(2,1)} %bitcast.3, bf16[4,128]{1,0:T(4,128)(2,1)} %cx_hbm.1, ...), custom_call_target="tpu_custom_call" | custom-call | tf_op jit(solution)/shard_map/pallas_call | solution.py:634
  62.9 1.9 %copy.13 = bf16[1,128,2048]{2,1,0:T(8,128)(2,1)} copy(bf16[1,128,2048]{2,1,0:T(8,128)(2,1)} %shard_map.109) | data formatting | bytes 1048576

commit v2 on v1

--- a/solution.py
+++ b/solution.py
@@ -13,8 +13,18 @@
 NORM_EPS = 1.0
 HALO = 8
 LANES = 128
-HOP = 2
-RELAYS = (8, 11, 14, 18)
+HOP = 4
+UP_SLOTS = (5, 7, 11, 16, 21, 23, 24, 26)
+BACK_SLOTS = (13, 16, 18, 20, 23, 25, 26, 28)
+UP_STATES = (2, 6, 11, 15, 19)
+BACK_STATES = (12, 14, 15, 16, 20)
+STATES_END = 23
+FINISH = 31
+RELAYS = (31, 34, 39, 45)
+LATER = 7
+LATE_SLOTS = (19, 20, 21, 22, 23, 25, 26, 28)
+BEHIND = 4
+CUBE = 4
 F32 = jnp.float32
 BF16 = jnp.bfloat16
 
@@ -41,7 +51,7 @@
     dl_hbm,
     gain_hbm,
     w_hbm,
-    out_ref,
+    out_hbm,
     raw_ref,
     dl_ref,
     cx_ref,
@@ -70,6 +80,7 @@
     wts,
     lasts,
     total,
+    rates,
     cact,
     local,
     a_in,
@@ -96,6 +107,8 @@
     two_recv,
     relay_send,
     relay_recv,
+    out_v,
+    out_send,
 ):
     tokens, inner_width = x_v.shape
     groups = b_v.shape[1] // STATE
@@ -109,7 +122,7 @@
     half_rows = rows // 2
     side = math.isqrt(dp // 2)
     cut = max(2, (3 * sp) // 8)
-    middle = cut + (sp - cut + 1) // 2
+    middle = cut + (sp - cut + 1) // 2 + (1 if sp > 8 else 0)
     reach = max(cut, sp - cut) - 1
 
     pos = lax.axis_index("sp")
@@ -137,7 +150,24 @@
         return ((line + dy + side) % side) * side + (column + dx + side) % side
 
     barrier = pltpu.get_barrier_semaphore()
-    greeted = [{"sp": (pos + j) % sp} for j in range(1, sp)] + [{"dp": partner}]
+    for j in range(1, sp):
+
+        @pl.when(pos + j < sp)
+        def _():
+            pl.semaphore_signal(
+                barrier,
+                inc=1,
+                device_id={"sp": (pos + j) % sp},
+                device_id_type=pl.DeviceIdType.MESH,
+            )
+
+    @pl.when(pos > 0)
+    def _():
+        pl.semaphore_signal(
+            barrier, inc=1, device_id={"sp": preceding}, device_id_type=pl.DeviceIdType.MESH
+        )
+
+    greeted = [{"dp": partner}]
     for axis in range(2):
         for i in range(1, side):
             greeted.append({"dp": 2 * chip(axis, i, 0) + core})
@@ -189,7 +219,7 @@
     for load in loads[3:]:
         load.wait()
     keep.wait()
-    pl.semaphore_wait(barrier, len(greeted))
+    pl.semaphore_wait(barrier, len(greeted) + jnp.minimum(pos + 1, sp - 1))
 
     halos = [
         remote(
@@ -207,18 +237,43 @@
         for copy in halos:
             copy.start()
 
-    shares = [
-        remote(
-            par.at[pos],
-            par.at[pos],
-            par_send.at[j - 1],
-            par_recv.at[j - 1],
-            {"sp": (pos + j) % sp},
-        )
-        for j in range(1, sp)
-    ]
-    for copy in shares:
-        copy.start()
+    def share(target):
+        return remote(
+            par.at[pos], par.at[pos], par_send.at[target], par_recv.at[pos], {"sp": target}
+        )
+
+    for j in range(1, sp):
+
+        @pl.when(pos >= j)
+        def _():
+            share((pos + sp - j) % sp).start()
+
+    @pl.when(pos < sp - 1)
+    def _():
+        share(following).start()
+
+    def early(source):
+        return (pos > 0) & (pos + 1 < source) & (source < cut)
+
+    def hear(source, now):
+        if not isinstance(now, bool):
+            now = now & (pos != source)
+        else:
+            now = (pos != source) & jnp.logical_not(early(source))
+
+        @pl.when(now)
+        def _():
+            remote(
+                par.at[source],
+                par.at[source],
+                par_send.at[source],
+                par_recv.at[source],
+                {"sp": source},
+            ).wait_recv()
+
+        @pl.when(now & (pos + 1 < source))
+        def _():
+            share(source).start()
 
     def stage_one(axis, i):
         return remote(
@@ -297,6 +352,10 @@
     def _():
         ext[:, 0:8, :] = jnp.zeros((groups, 8, ext.shape[2]), F32)
 
+    causal_ones = jnp.where(causal, 1.0, 0.0).astype(F32)
+    steps_sum = dot(causal_ones, dt, lax.Precision.HIGHEST)
+    rates[...] = jnp.zeros(rates.shape, F32)
+
     @pl.when((pos == 0) | (pos == cut))
     def _():
         a_in[...] = jnp.zeros(a_in.shape, BF16)
@@ -330,44 +389,34 @@
         b_ts[g] = b_t
         scores[g] = dot(c_act, b_t)
 
-    for copy in shares:
-        copy.wait_recv()
-    gathered = par[0].astype(F32)
-    for s in range(1, sp):
-        gathered = gathered + par[s].astype(F32)
-    rates = gathered[tap_count : tap_count + 1, :]
-    for i in range(1, 3):
-        rates = rates + gathered[tap_count + i : tap_count + i + 1, :]
-    log_decay = dt * (-jnp.exp(rates))
-    cum = dot(jnp.where(causal, 1.0, 0.0).astype(F32), log_decay, lax.Precision.HIGHEST)
-    cum_t = jnp.transpose(cum)
-    last = cum[tokens - 1 : tokens, :]
-    lasts[0] = jnp.broadcast_to(last, lasts.shape[1:])
-    tail = dt * jnp.exp(last - cum)
-
-    def tell(d):
+    def ranked(center):
+        near = lambda g: abs((g + 0.5) * per - center)
+        return sorted(range(groups), key=near)
+
+    def staged(order):
+        single = min(4, groups - 1)
+        return [[g] for g in order[:single]] + [order[single:]]
+
+    per = group_width // tap_width
+    back_order = ranked(cut + 1.2)
+    up_stages, back_stages = staged(list(range(groups))), staged(back_order)
+    stages = len(up_stages)
+
+    def back_group(k):
+        g = jnp.int32(back_order[0])
+        for i in range(1, groups):
+            g = jnp.where(k == i, back_order[i], g)
+        return g
+
+    def tell(d, i):
         target = jnp.where(first, pos + sp - d, pos + d) % sp
         return remote(
-            lasts.at[0], lasts.at[d], last_send.at[d], last_recv.at[d], {"sp": target}
-        )
-
-    def tells(d):
-        return (first & (pos >= d)) | (jnp.logical_not(first) & (pos + d < sp))
-
-    def hears(d):
-        return (first & (pos + d < cut)) | (jnp.logical_not(first) & (pos - d >= cut))
-
-    for d in range(1, reach + 1):
-
-        @pl.when(tells(d))
-        def _():
-            tell(d).start()
-
-    for chunk in range(chunks):
-        begin = chunk * LANES
-        g, at = begin // group_width, begin % group_width
-        s = begin // tap_width
-        taps[g, 0:tap_count, at : at + LANES] = par[s].astype(F32)[0:tap_count, :]
+            lasts.at[0, i], lasts.at[d, i], last_send.at[d, i], last_recv.at[d, i], {"sp": target}
+        )
+
+    def tells(d, i):
+        later = jnp.logical_not(first) & (pos + d < sp)
+        return (first & (pos >= d)) | (later if i == stages - 1 else False)
 
     def chain(j):
         return remote(a_out.at[j], a_in.at[j], a_send.at[j], a_recv.at[j], {"sp": following})
@@ -396,7 +445,7 @@
     def spread_columns(values, h):
         return jnp.where(left_half, values[:, h : h + 1], values[:, h + 1 : h + 2])
 
-    def states(g):
+    def states(g, tail):
         b_t = b_ts[g]
         for p in range(pairs):
             j = g * pairs + p
@@ -405,38 +454,29 @@
             x_tail = (x_act.astype(F32) * spread_columns(tail, 2 * j)).astype(BF16)
             local[j] = dot(b_t, x_tail)
 
-    def begin_flows(some, which):
-        @pl.when((core == which) & ((pos == 0) | (pos == cut)))
+    def begin_flows(some):
+        @pl.when((pos == 0) | (pos == cut))
         def _():
             for g in some:
                 for j in range(g * pairs, (g + 1) * pairs):
                     a_out[j] = local[j].astype(BF16)
                     chain(j).start()
 
-        @pl.when((core == which) & (pos == cut - 1))
+        @pl.when(pos == cut - 1)
         def _():
             for g in some:
                 for j in range(g * pairs, (g + 1) * pairs):
                     b_out[j] = local[j].astype(BF16)
                     back(j).start()
 
-    for number, some in enumerate(([0], range(1, groups // 2), range(groups // 2, groups))):
-        for g in some:
-            states(g)
-        if number == 0:
-            spread_rows(elast, jnp.exp(last))
-        begin_flows(some, 0)
-
-    def weigh():
+    def weigh(stage, count):
         total[...] = jnp.zeros(total.shape, F32)
-        for d in range(1, reach + 1):
-
-            @pl.when(hears(d))
+        for d in range(1, count + 1):
+
+            @pl.when(jnp.where(first, pos + d < cut, pos - d >= cut))
             def _():
-                tell(d).wait_recv()
-                total[...] += lasts[d]
-
-        spread_rows(wts, jnp.exp(total[0:1, :]))
+                tell(d, stage).wait_recv()
+                total[...] += lasts[d, stage]
 
     def step_a(j):
         @pl.when((pos != 0) & (pos != cut))
@@ -474,23 +514,126 @@
             def _():
                 carry_down(j).start()
 
-    lag_a = jnp.where(first, HOP * pos, HOP * (pos - cut))
-    lag_b = jnp.where(
+    def find(s, slots):
+        k = jnp.int32(-1)
+        for i, at in enumerate(slots):
+            k = jnp.where(s == at, i, k)
+        return k
+
+    cube = pos // CUBE
+    base_a = jnp.where(first, HOP * pos + cube, HOP * (pos - cut) + cube - cut // CUBE)
+    lower = jnp.logical_not(first) & (pos < middle)
+    upper = pos >= middle
+    last_cube = (cut - 1) // CUBE
+    base_b = jnp.where(
         first,
-        HOP * (cut - 1 - pos),
-        jnp.where(pos < middle, HOP * pos, HOP * (cut + sp - 1 - pos)),
+        HOP * (cut - 1 - pos) + jnp.where(pos < CUBE, BEHIND, 0) + last_cube - cube,
+        jnp.where(
+            lower,
+            HOP * pos + cube,
+            HOP * (cut + sp - 1 - pos) + last_cube + 1 + (sp - 1) // CUBE - cube,
+        ),
     )
+    slots_a = [
+        base_a
+        + jnp.where(
+            first, UP_SLOTS[k], jnp.where(pos > cut + 1, LATE_SLOTS[k], BACK_SLOTS[k])
+        )
+        for k in range(groups)
+    ]
+    slots_b = [
+        base_b + jnp.where(lower, UP_SLOTS[k], BACK_SLOTS[k]) for k in range(groups)
+    ]
 
     def flows(s):
-        @pl.when((s >= lag_a) & (s < lag_a + groups))
-        def _():
+        k_a = find(s, slots_a)
+
+        @pl.when(k_a >= 0)
+        def _():
+            g = jnp.where(first, k_a, back_group(k_a))
             for p in range(pairs):
-                step_a((s - lag_a) * pairs + p)
-
-        @pl.when((s >= lag_b) & (s < lag_b + groups))
-        def _():
+                step_a(g * pairs + p)
+
+        k_b = find(s, slots_b)
+
+        @pl.when(k_b >= 0)
+        def _():
+            g = jnp.where(lower, k_b, back_group(k_b))
+
+            @pl.when(pos < cut - 1)
+            def _():
+                @pl.when(k_b < stages)
+                def _():
+                    weigh(k_b, cut - 1)
+
+                weight = jnp.exp(total[...])
+                for p in range(pairs):
+                    j = g * pairs + p
+                    moved = pltpu.roll(weight, (LANES - 2 * j) % LANES, 1)
+                    wts[j, 0:1, :] = jnp.where(left_row, moved[0:1, 0:1], moved[0:1, 1:2])
+
             for p in range(pairs):
-                step_b((s - lag_b) * pairs + p)
+                step_b(g * pairs + p)
+
+    def flow_slot(s, carry):
+        flows(s)
+        return carry
+
+    def decayed():
+        rate = -jnp.exp(rates[0:1, :])
+        cum = steps_sum * rate
+        return cum, cum[tokens - 1 : tokens, :]
+
+    def make_states(parts, at, lines_after):
+        begun, known, told = 0, set(), set()
+        for number, some in enumerate(parts):
+            lax.fori_loop(begun, at[number], flow_slot, 0)
+            begun = at[number]
+            sum_rates = rates[0:1, :]
+            sources = [g * per + i for g in some for i in range(per)]
+            for source in sorted(sources, key=lambda d: d < cut):
+                hear(source, True)
+            for g in some:
+                for i in range(per):
+                    source = g * per + i
+                    gathered = par[source].astype(F32)
+                    taps[g, 0:tap_count, i * tap_width : (i + 1) * tap_width] = gathered[
+                        0:tap_count, :
+                    ]
+                    for part in range(3):
+                        sum_rates = sum_rates + gathered[tap_count + part : tap_count + part + 1, :]
+            rates[0:1, :] = sum_rates
+            cum, last = decayed()
+            tail = dt * jnp.exp(last - cum)
+            decay = jnp.exp(last)
+            for g in some:
+                if g != some[0]:
+                    lax.fori_loop(begun, begun + 1, flow_slot, 0)
+                    begun += 1
+                states(g, tail)
+                for j in range(g * pairs, (g + 1) * pairs):
+                    elast[j, 0:1, :] = jnp.where(
+                        left_row, decay[:, 2 * j : 2 * j + 1], decay[:, 2 * j + 1 : 2 * j + 2]
+                    )
+                begin_flows([g])
+            known |= set(some)
+            for i, needed in enumerate(back_stages):
+                if i not in told and set(needed) <= known:
+                    told.add(i)
+                    lasts[0, i] = jnp.broadcast_to(last, lasts.shape[2:])
+                    for d in range(1, reach + 1):
+
+                        @pl.when(tells(d, i))
+                        def _():
+                            tell(d, i).start()
+
+            if number == lines_after:
+
+                @pl.when(pos <= cut + 1)
+                def _():
+                    spread_lines()
+
+        lax.fori_loop(begun, STATES_END, flow_slot, 0)
 
     def inside(g):
         for p in range(pairs):
@@ -508,18 +651,38 @@
             inner[g, :, local_columns] = jnp.where(left_half, parts[0], parts[1])
             ecum[g, :, local_columns] = jnp.exp(jnp.where(left_half, spread[0], spread[1]))
 
-    for s in range(groups):
-        if s == 0 or s == groups // 2:
-
-            @pl.when(first & ((pos >= cut - 2) if s == 0 else (pos < cut - 2)))
-            def _():
-                weigh()
-
-        flows(s)
-        inside(s)
-        if s == 0:
-            spread_lines()
-    begin_flows(range(groups), 1)
+    for source in range(3, cut):
+        hear(source, early(source))
+
+    @pl.when(pos > cut + 1)
+    def _():
+        spread_lines()
+
+    near = (2 * cut) // 3
+
+    @pl.when(pos < near)
+    def _():
+        make_states(up_stages, UP_STATES, min(2, stages - 1))
+
+    @pl.when(pos >= near)
+    def _():
+        make_states(back_stages, BACK_STATES, min(3, stages - 1))
+
+    cum, _ = decayed()
+    cum_t = jnp.transpose(cum)
+
+    @pl.when(first)
+    def _():
+        lax.fori_loop(STATES_END, FINISH, flow_slot, 0)
+
+    @pl.when(jnp.logical_not(first))
+    def _():
+        for part in range(4):
+            for g in range(part * groups // 4, (part + 1) * groups // 4):
+                inside(g)
+            begun = STATES_END + 2 * part
+            lax.fori_loop(begun, begun + 2, flow_slot, 0)
+
 
     sum_down = lax.broadcasted_iota(jnp.int32, (group_width, group_width), 0) // HEAD_DIM
     sum_across = lax.broadcasted_iota(jnp.int32, (group_width, group_width), 1) // HEAD_DIM
@@ -541,28 +704,77 @@
         gain = gain_ref[0:1, pl.ds(pl.multiple_of(g * group_width, group_width), group_width)]
         normed[g] = (value * lax.rsqrt(mean + NORM_EPS) * gain).astype(BF16)
 
-    lag_f = jnp.maximum(jnp.maximum(lag_a, lag_b), groups)
-    slots = jnp.maximum(lag_f + groups, RELAYS[side - 1] + 1)
+    slots_f = []
+    for k in range(groups):
+        both = jnp.maximum(slots_a[k], slots_b[k])
+        after = jnp.maximum(slots_a[-1] + 1 + k, slots_b[k])
+        needed = jnp.where(lower, after, both)
+        slots_f.append(jnp.maximum(needed, FINISH + k))
+    later = jnp.where(first, 0, LATER)
+    ends = [jnp.where(first, 0, slots_f[-1]), slots_a[-1], slots_b[-1], RELAYS[side - 1] + later + 2]
+    end = ends[0]
+    for other in ends[1:]:
+        end = jnp.maximum(end, other)
 
     def slot(s, carry):
         flows(s)
         for step, at in enumerate(RELAYS[:side]):
 
-            @pl.when(s == at)
+            @pl.when(s == at + later)
             def _():
                 pass_rows(step)
 
-        @pl.when(jnp.logical_not(first) & (s == lag_f))
-        def _():
-            weigh()
-
-        @pl.when((s >= lag_f) & (s < lag_f + groups))
-        def _():
-            finish(s - lag_f)
+        @pl.when(s == RELAYS[side - 1] + later + 2)
+        def _():
+            for axis in range(2):
+                for i in steps:
+                    for k in range(side):
+                        stage_two(axis, k, i).wait_send()
+                for k in range(side):
+                    for i in range(side):
+                        if k or i:
+                            relay(axis, k, i).wait_send()
+
+        @pl.when(jnp.logical_not(first) & (s == slots_f[0]))
+        def _():
+            weigh(stages - 1, reach)
+            spread_rows(wts, jnp.exp(total[0:1, :]))
+
+        k_f = find(s, slots_f)
+
+        @pl.when(jnp.logical_not(first) & (k_f >= 0))
+        def _():
+            finish(jnp.where(upper, back_group(k_f), k_f))
 
         return carry
 
-    lax.fori_loop(groups, slots, slot, 0)
+    for j in range(1, sp):
+        share((pos + j) % sp).wait_send()
+
+    @pl.when(pos < sp - 1)
+    def _():
+        for copy in halos:
+            copy.wait_send()
+
+    for i in range(stages):
+        for d in range(1, reach + 1):
+
+            @pl.when(tells(d, i))
+            def _():
+                tell(d, i).wait_send()
+
+    own.wait_send()
+    for axis in range(2):
+        for i in steps:
+            stage_one(axis, i).wait_send()
+
+    lax.fori_loop(FINISH, end + 1, slot, 0)
+
+    @pl.when(first)
+    def _():
+        for g in range(groups):
+            inside(g)
+            finish(g)
 
     own.wait_recv()
     for axis in range(2):
@@ -570,33 +782,23 @@
             for i in range(side):
                 if k or i:
                     relay(axis, k, i).wait_recv()
-    result = dot(normed[0], w_all[0:group_width, :])
-    for g in range(1, groups):
-        result += dot(normed[g], w_all[g * group_width : (g + 1) * group_width, :])
-    out_ref[0] = result.astype(BF16)
-
-    own.wait_send()
-    for copy in shares:
-        copy.wait_send()
-    for axis in range(2):
-        for i in steps:
-            stage_one(axis, i).wait_send()
-            for k in range(side):
-                stage_two(axis, k, i).wait_send()
-        for k in range(side):
-            for i in range(side):
-                if k or i:
-                    relay(axis, k, i).wait_send()
-    for d in range(1, reach + 1):
-
-        @pl.when(tells(d))
-        def _():
-            tell(d).wait_send()
+    blocks = out_send.shape[0]
+    width = out_v.shape[1] // blocks
+    outs = []
+    for block in range(blocks):
+        columns = slice(block * width, (block + 1) * width)
+        result = dot(normed[0], w_all[0:group_width, columns])
+        for g in range(1, groups):
+            result += dot(normed[g], w_all[g * group_width : (g + 1) * group_width, columns])
+        out_v[:, columns] = result.astype(BF16)
+        copy = pltpu.make_async_copy(
+            out_v.at[:, columns], out_hbm.at[0, :, columns], out_send.at[block]
+        )
+        copy.start()
+        outs.append(copy)
 
     @pl.when(pos < sp - 1)
     def _():
-        for copy in halos:
-            copy.wait_send()
         for j in range(chunks):
             chain(j).wait_send()
 
@@ -604,6 +806,9 @@
     def _():
         for j in range(chunks):
             back(j).wait_send()
+
+    for copy in outs:
+        copy.wait()
 
 
 def body(
@@ -626,16 +831,16 @@
     groups = state_width // STATE
     group_width = width // groups
     chunks = width // LANES
+    stages = min(4, groups - 1) + 1
     columns = w_out.shape[1]
     side = math.isqrt(dp // 2)
-    vmem = pl.BlockSpec(memory_space=pltpu.VMEM)
     anywhere = pl.BlockSpec(memory_space=pl.ANY)
     dma = pltpu.SemaphoreType.DMA
     return pl.pallas_call(
         functools.partial(kernel, sp, dp),
         out_shape=jax.ShapeDtypeStruct((1, tokens, columns), BF16),
         in_specs=[anywhere] * 11,
-        out_specs=vmem,
+        out_specs=anywhere,
         scratch_shapes=[
             pltpu.VMEM((step_raw.shape[2], tokens), BF16),
             pltpu.VMEM((1, decay_log.shape[0]), F32),
@@ -663,7 +868,8 @@
             pltpu.VMEM((groups, tokens, group_width), F32),
             pltpu.VMEM((chunks, 8, LANES), F32),
             pltpu.VMEM((chunks, 8, LANES), F32),
-            pltpu.VMEM((sp, 8, LANES), F32),
+            pltpu.VMEM((sp, stages, 8, LANES), F32),
+            pltpu.VMEM((8, LANES), F32),
             pltpu.VMEM((8, LANES), F32),
             pltpu.VMEM((groups, tokens, STATE), BF16),
             pltpu.VMEM((chunks, STATE, LANES), F32),
@@ -676,8 +882,8 @@
             dma((11,)),
             dma((sp,)),
             dma((sp,)),
-            dma((sp,)),
-            dma((sp,)),
+            dma((sp, stages)),
+            dma((sp, stages)),
             dma((3,)),
             dma((3,)),
             dma((chunks,)),
@@ -691,6 +897,8 @@
             dma((2, side, side)),
             dma((2, side, side)),
             dma((2, side, side)),
+            pltpu.VMEM((tokens, columns), BF16),
+            dma((2,)),
         ],
         compiler_params=pltpu.CompilerParams(
             collective_id=0, has_side_effects=True, vmem_limit_bytes=60 * 1024 * 1024

time: 65 us -> 64.4 us (level)
  the two profiles are of different devices: /device:TPU:356 before, /device:TPU:480 now
where the time goes in v2:
time: 64.4 us; the launch traced here: 64.1 us
  Pallas kernels  62.2 us (97%)
  local copies, waits for them, and re-layouts  1.88 us (3%)
    pallas_call x1, Pallas kernels, body(): pl.pallas_call(functools.partial(kernel, sp, dp), out_shape=jax.ShapeDtyp...  62.2 us
    unnamed x1, local copies, waits for them, and re-layouts  1.88 us

profile of v2, /device:TPU:480, one launch (start us, length us, event | category | flops | bytes accessed | tf_op | source)
XLA Modules:
  0.0 64.1 jit_solution(12561178170375252741)
XLA Ops:
  0.0 62.2 %shard_map.109 = bf16[1,128,2048]{2,1,0:T(8,128)(2,1)} custom-call(bf16[1,128,2048]{2,1,0:T(8,128)(2,1)} %x_hbm.1, bf16[1,128,1024]{2,1,0:T(8,128)(2,1)} %b_hbm.1, bf16[1,128,1024]{2,1,0:T(8,128)(2,1)} %c_hbm.1, bf16[1,128,2048]{2,1,0:T(8,128)(2,1)} %z_hbm.1, bf16[1,32,128]{2,1,0:T(8,128)(2,1)} %bitcast.3, bf16[4,128]{1,0:T(4,128)(2,1)} %cx_hbm.1, ...), custom_call_target="tpu_custom_call" | custom-call | tf_op jit(solution)/shard_map/pallas_call | solution.py:839
  62.2 1.9 %copy.13 = bf16[1,128,2048]{2,1,0:T(8,128)(2,1)} copy(bf16[1,128,2048]{2,1,0:T(8,128)(2,1)} %shard_map.109) | data formatting | bytes 1048576

commit v3 on v2

--- a/solution.py
+++ b/solution.py
@@ -239,7 +239,7 @@
 
     def share(target):
         return remote(
-            par.at[pos], par.at[pos], par_send.at[target], par_recv.at[pos], {"sp": target}
+            par.at[pos], par.at[pos], par_send.at[0], par_recv.at[pos], {"sp": target}
         )
 
     for j in range(1, sp):
@@ -266,7 +266,7 @@
             remote(
                 par.at[source],
                 par.at[source],
-                par_send.at[source],
+                par_send.at[0],
                 par_recv.at[source],
                 {"sp": source},
             ).wait_recv()
@@ -279,8 +279,8 @@
         return remote(
             piece(axis, 0, 0),
             piece(axis, 0, 0),
-            one_send.at[axis, i],
-            one_recv.at[axis, i],
+            one_send.at[0],
+            one_recv.at[axis, i - 1],
             {"dp": 2 * chip(axis, i, 0) + core},
         )
 
@@ -288,8 +288,8 @@
         return remote(
             piece(axis, -k, 0),
             piece(axis, -k, 0),
-            two_send.at[axis, k, i],
-            two_recv.at[axis, k, i],
+            two_send.at[0],
+            two_recv.at[axis, k, i - 1],
             {"dp": 2 * chip(axis, 0, i) + core},
         )
 
@@ -297,8 +297,8 @@
         return remote(
             piece(axis, -k, -i),
             piece(axis, -k, -i),
-            relay_send.at[axis, k, i],
-            relay_recv.at[axis, k, i],
+            relay_send.at[0],
+            relay_recv.at[0],
             {"dp": partner},
         )
 
@@ -411,7 +411,7 @@
     def tell(d, i):
         target = jnp.where(first, pos + sp - d, pos + d) % sp
         return remote(
-            lasts.at[0, i], lasts.at[d, i], last_send.at[d, i], last_recv.at[d, i], {"sp": target}
+            lasts.at[0, i], lasts.at[d, i], last_send.at[d - 1, i], last_recv.at[d - 1, i], {"sp": target}
         )
 
     def tells(d, i):
@@ -419,19 +419,19 @@
         return (first & (pos >= d)) | (later if i == stages - 1 else False)
 
     def chain(j):
-        return remote(a_out.at[j], a_in.at[j], a_send.at[j], a_recv.at[j], {"sp": following})
+        return remote(a_out.at[j], a_in.at[j], a_send.at[0], a_recv.at[j], {"sp": following})
 
     def cross(j):
-        return remote(a_out.at[j], b_in.at[j], a_send.at[j], b_recv.at[j], {"sp": following})
+        return remote(a_out.at[j], b_in.at[j], a_send.at[0], b_recv.at[j], {"sp": following})
 
     def back(j):
-        return remote(b_out.at[j], b_in.at[j], b_send.at[j], b_recv.at[j], {"sp": preceding})
+        return remote(b_out.at[j], b_in.at[j], b_send.at[0], b_recv.at[j], {"sp": preceding})
 
     def carry_up(j):
-        return remote(b_in.at[j], b_in.at[j], b_send.at[j], b_recv.at[j], {"sp": following})
+        return remote(b_in.at[j], b_in.at[j], b_send.at[0], b_recv.at[j], {"sp": following})
 
     def carry_down(j):
-        return remote(b_in.at[j], b_in.at[j], b_send.at[j], b_recv.at[j], {"sp": preceding})
+        return remote(b_in.at[j], b_in.at[j], b_send.at[0], b_recv.at[j], {"sp": preceding})
 
     carries_up = (pos >= cut) & (pos < middle - 1)
     carries_down = pos > middle
@@ -726,14 +726,9 @@
 
         @pl.when(s == RELAYS[side - 1] + later + 2)
         def _():
-            for axis in range(2):
-                for i in steps:
-                    for k in range(side):
-                        stage_two(axis, k, i).wait_send()
-                for k in range(side):
-                    for i in range(side):
-                        if k or i:
-                            relay(axis, k, i).wait_send()
+            if side > 1:
+                many(twos, two_send.at[0], two_recv.at[0, 0, 0]).wait_send()
+                many(relays, relay_send.at[0], relay_recv.at[0]).wait_send()
 
         @pl.when(jnp.logical_not(first) & (s == slots_f[0]))
         def _():
@@ -748,8 +743,8 @@
 
         return carry
 
-    for j in range(1, sp):
-        share((pos + j) % sp).wait_send()
+    shared = par.at[pl.ds(0, sp - 1)]
+    remote(shared, shared, par_send.at[0], par_recv.at[0], {"sp": following}).wait_send()
 
     @pl.when(pos < sp - 1)
     def _():
@@ -763,10 +758,14 @@
             def _():
                 tell(d, i).wait_send()
 
+    def many(count, send, recv):
+        some = w_all.at[pl.ds(0, count * half_rows), :]
+        return remote(some, some, send, recv, {"dp": partner})
+
     own.wait_send()
-    for axis in range(2):
-        for i in steps:
-            stage_one(axis, i).wait_send()
+    ones, twos, relays = 2 * (side - 1), 2 * side * (side - 1), 2 * (side * side - 1)
+    if side > 1:
+        many(ones, one_send.at[0], one_recv.at[0, 0]).wait_send()
 
     lax.fori_loop(FINISH, end + 1, slot, 0)
 
@@ -777,11 +776,8 @@
             finish(g)
 
     own.wait_recv()
-    for axis in range(2):
-        for k in range(side):
-            for i in range(side):
-                if k or i:
-                    relay(axis, k, i).wait_recv()
+    if side > 1:
+        many(relays, relay_send.at[0], relay_recv.at[0]).wait_recv()
     blocks = out_send.shape[0]
     width = out_v.shape[1] // blocks
     outs = []
@@ -799,13 +795,11 @@
 
     @pl.when(pos < sp - 1)
     def _():
-        for j in range(chunks):
-            chain(j).wait_send()
+        remote(a_out, a_in, a_send.at[0], a_recv.at[0], {"sp": following}).wait_send()
 
     @pl.when(first | carries_up | carries_down)
     def _():
-        for j in range(chunks):
-            back(j).wait_send()
+        remote(b_out, b_in, b_send.at[0], b_recv.at[0], {"sp": preceding}).wait_send()
 
     for copy in outs:
         copy.wait()
@@ -832,6 +826,8 @@
     group_width = width // groups
     chunks = width // LANES
     stages = min(4, groups - 1) + 1
+    cut = max(2, (3 * sp) // 8)
+    reach = max(cut, sp - cut) - 1
     columns = w_out.shape[1]
     side = math.isqrt(dp // 2)
     anywhere = pl.BlockSpec(memory_space=pl.ANY)
@@ -880,23 +876,23 @@
             pltpu.VMEM((groups, tokens, group_width), BF16),
             pltpu.VMEM((width, columns), BF16),
             dma((11,)),
+            dma((1,)),
             dma((sp,)),
-            dma((sp,)),
-            dma((sp, stages)),
-            dma((sp, stages)),
+            dma((reach, stages)),
+            dma((reach, stages)),
             dma((3,)),
             dma((3,)),
+            dma((1,)),
             dma((chunks,)),
-            dma((chunks,)),
-            dma((chunks,)),
+            dma((1,)),
             dma((chunks,)),
             dma((2,)),
-            dma((2, side)),
-            dma((2, side)),
-            dma((2, side, side)),
-            dma((2, side, side)),
-            dma((2, side, side)),
-            dma((2, side, side)),
+            dma((1,)),
+            dma((2, max(1, side - 1))),
+            dma((1,)),
+            dma((2, side, max(1, side - 1))),
+            dma((1,)),
+            dma((1,)),
             pltpu.VMEM((tokens, columns), BF16),
             dma((2,)),
         ],

time: 64.4 us -> 62.3 us (0.967)
  Pallas kernels: 62.2 us -> 59.9 us
    pallas_call x1, Pallas kernels: 62.2 us -> 59.9 us  [body(): pl.pallas_call(functools.partial(kernel, sp, dp), out_shape=jax.ShapeDtyp...]
where the time goes in v3:
time: 62.3 us; the launch traced here: 61.8 us
  Pallas kernels  59.9 us (96%)
  local copies, waits for them, and re-layouts  1.88 us (3%)
    pallas_call x1, Pallas kernels, body(): pl.pallas_call(functools.partial(kernel, sp, dp), out_shape=jax.ShapeDtyp...  59.9 us
    unnamed x1, local copies, waits for them, and re-layouts  1.88 us

profile of v3, /device:TPU:480, one launch (start us, length us, event | category | flops | bytes accessed | tf_op | source)
XLA Modules:
  0.0 61.8 jit_solution(9506647282821095991)
XLA Ops:
  0.0 59.9 %shard_map.109 = bf16[1,128,2048]{2,1,0:T(8,128)(2,1)} custom-call(bf16[1,128,2048]{2,1,0:T(8,128)(2,1)} %x_hbm.1, bf16[1,128,1024]{2,1,0:T(8,128)(2,1)} %b_hbm.1, bf16[1,128,1024]{2,1,0:T(8,128)(2,1)} %c_hbm.1, bf16[1,128,2048]{2,1,0:T(8,128)(2,1)} %z_hbm.1, bf16[1,32,128]{2,1,0:T(8,128)(2,1)} %bitcast.3, bf16[4,128]{1,0:T(4,128)(2,1)} %cx_hbm.1, ...), custom_call_target="tpu_custom_call" | custom-call | tf_op jit(solution)/shard_map/pallas_call | solution.py:835
  60.0 1.9 %copy.13 = bf16[1,128,2048]{2,1,0:T(8,128)(2,1)} copy(bf16[1,128,2048]{2,1,0:T(8,128)(2,1)} %shard_map.109) | data formatting | bytes 1048576

commit v4 on v3

--- a/solution.py
+++ b/solution.py
@@ -253,7 +253,8 @@
         share(following).start()
 
     def early(source):
-        return (pos > 0) & (pos + 1 < source) & (source < cut)
+        among_first = (pos > 0) & (source < cut)
+        return (pos + 1 < source) & (among_first | (pos > cut + 1))
 
     def hear(source, now):
         if not isinstance(now, bool):
@@ -534,10 +535,11 @@
             HOP * (cut + sp - 1 - pos) + last_cube + 1 + (sp - 1) // CUBE - cube,
         ),
     )
+    after_sums = jnp.where(pos > middle, 4, 0)
     slots_a = [
         base_a
         + jnp.where(
-            first, UP_SLOTS[k], jnp.where(pos > cut + 1, LATE_SLOTS[k], BACK_SLOTS[k])
+            first, UP_SLOTS[k], jnp.where(pos > cut + 1, LATE_SLOTS[k] + after_sums, BACK_SLOTS[k])
         )
         for k in range(groups)
     ]
@@ -657,6 +659,9 @@
     @pl.when(pos > cut + 1)
     def _():
         spread_lines()
+
+    for source in range(cut + 4, sp):
+        hear(source, early(source))
 
     near = (2 * cut) // 3
 

time: 62.3 us -> 62 us (level)
  no operation moved by 1% of the time
where the time goes in v4:
time: 62 us; the launch traced here: 61.8 us
  Pallas kernels  59.9 us (97%)
  local copies, waits for them, and re-layouts  1.88 us (3%)
    pallas_call x1, Pallas kernels, body(): pl.pallas_call(functools.partial(kernel, sp, dp), out_shape=jax.ShapeDtyp...  59.9 us
    unnamed x1, local copies, waits for them, and re-layouts  1.88 us

profile of v4, /device:TPU:480, one launch (start us, length us, event | category | flops | bytes accessed | tf_op | source)
XLA Modules:
  0.0 61.8 jit_solution(4351971707863203845)
XLA Ops:
  0.0 59.9 %shard_map.109 = bf16[1,128,2048]{2,1,0:T(8,128)(2,1)} custom-call(bf16[1,128,2048]{2,1,0:T(8,128)(2,1)} %x_hbm.1, bf16[1,128,1024]{2,1,0:T(8,128)(2,1)} %b_hbm.1, bf16[1,128,1024]{2,1,0:T(8,128)(2,1)} %c_hbm.1, bf16[1,128,2048]{2,1,0:T(8,128)(2,1)} %z_hbm.1, bf16[1,32,128]{2,1,0:T(8,128)(2,1)} %bitcast.3, bf16[4,128]{1,0:T(4,128)(2,1)} %cx_hbm.1, ...), custom_call_target="tpu_custom_call" | custom-call | tf_op jit(solution)/shard_map/pallas_call | solution.py:840
  59.9 1.9 %copy.13 = bf16[1,128,2048]{2,1,0:T(8,128)(2,1)} copy(bf16[1,128,2048]{2,1,0:T(8,128)(2,1)} %shard_map.109) | data formatting | bytes 1048576
